TPU v7x, 1024 devices: a whole 4x8x16 slice. The times are simulated.
1024 devices in a mesh: ep: 32 (over z, core), tp: 32 (over y, x).
Axes of the slice: x: 4, y: 8, z: 16, core: 2. Of those that a mesh axis runs over, the one named last changes fastest.
Arguments:
- tokens: bfloat16 [6144, 4096], P('ep'), may hold values from -6 to 6
- expert_ids: int32 [6144, 2], P('ep'), may hold values from 0 to 31, all different within a row; in each aligned block of 192 rows (0 to 191, 192 to 383, ...) at most 15 rows name the same one
- route_weight: float32 [6144, 2], P('ep'), may hold values from 0.1 to 1
- norm_gain: float32 [4096], replicated, may hold values from 0.1 to 1.9
- gate_weight: bfloat16 [32, 4096, 4096], P('ep', None, 'tp'), may hold values from -0.28125 to 0.28125
- up_weight: bfloat16 [32, 4096, 4096], P('ep', None, 'tp'), may hold values from -0.28125 to 0.28125
- down_weight: bfloat16 [32, 4096, 4096], P('ep', None, 'tp'), may hold values from -0.028076172 to 0.028076172
Outputs:
- mixed: bfloat16 [6144, 4096], P('ep', 'tp')
Inputs may be any that keep to these rules, and one draw needn't show every extreme that they name: `expert_ids`: each row names 2 different experts. In each aligned block of 192 rows (the tokens of one index of ep) no expert is named by more than 15 rows, and in some block some expert is named by exactly 15 rows.
All inputs are finite; a program needn't handle non-finite values.
Results may differ from a plain program's by a relative error of at most 0.007.
Values may be sent and summed in bfloat16 or wider, within the bound.
No kernel may reach another device: no remote copies, remote signals or barrier semaphores. Data moves between devices by JAX's collectives and lax.ppermute only.
A program may use at most 32 MiB of HBM per device.

v0:
```python
import jax
import jax.numpy as jnp
from jax import lax
from jax.experimental import pallas as pl
from jax.experimental.pallas import tpu as pltpu
from jax.sharding import Mesh
from jax.sharding import PartitionSpec as P


EPS = 1e-06
LIMIT = 7.0
ALPHA = 1.702
F32 = jnp.float32
BF16 = jnp.bfloat16

VMEM = pl.BlockSpec(memory_space=pltpu.VMEM)
SMEM = pl.BlockSpec(memory_space=pltpu.SMEM)
HBM = pl.BlockSpec(memory_space=pltpu.HBM)


def params(mib):
    return pltpu.CompilerParams(vmem_limit_bytes=mib << 20)


def swap(x, axes):
    return lax.all_to_all(x, axes, split_axis=0, concat_axis=0, tiled=True)


def shifted(n, by):
    return [(i, (i + by) % n) for i in range(n)]


def weight_quarters(x_at, gate_weight, up_weight, down_weight, nx):
    width, ff = gate_weight.shape
    ny, _, _, cols = down_weight.shape
    rows = width // nx

    def kernel(at, gate, up, down, *refs):
        outs, sem = refs[: 2 * nx], refs[2 * nx]
        copies = []
        for s in range(nx):
            quarter = lax.rem(at[0] + s, nx)
            for side, src in enumerate((gate, up)):
                copies.append(
                    pltpu.make_async_copy(
                        src.at[pl.ds(quarter * rows, rows)],
                        outs[s].at[:, pl.ds(side * ff, ff)],
                        sem.at[3 * s + side],
                    )
                )
            copies.append(pltpu.make_async_copy(down.at[:, quarter], outs[nx + s], sem.at[3 * s + 2]))
        for copy in copies:
            copy.start()
        for copy in copies:
            copy.wait()

    return pl.pallas_call(
        kernel,
        out_shape=[jax.ShapeDtypeStruct((rows, 2 * ff), BF16)] * nx
        + [jax.ShapeDtypeStruct((ny, ff, cols), BF16)] * nx,
        in_specs=[SMEM, HBM, HBM, HBM],
        out_specs=[VMEM] * (2 * nx),
        scratch_shapes=[pltpu.SemaphoreType.DMA((3 * nx,))],
        compiler_params=params(4),
        name="weight_quarters",
    )(x_at, gate_weight, up_weight, down_weight)


def dispatch(tp_at, tokens, ids, gain, experts, room, cols):
    rows, width = tokens.shape
    top = ids.shape[0]
    slots = experts * room

    def kernel(at, tok, ids_ref, gain_ref, out, dest_ref):
        values = tok[...].astype(F32)
        scale = lax.rsqrt(jnp.sum(values * values, axis=-1, keepdims=True) * (1.0 / width) + EPS)
        start = pl.multiple_of(at[0] * cols, cols)
        own = (tok[:, pl.ds(start, cols)].astype(F32) * scale * gain_ref[:, pl.ds(start, cols)]).astype(BF16)
        expert = lax.broadcasted_iota(jnp.int32, (experts, rows), 0)
        here = [ids_ref[k : k + 1, :] == expert for k in range(top)]
        named = sum(h.astype(F32) for h in here).astype(BF16)
        earlier = lax.broadcasted_iota(jnp.int32, (rows, rows), 0) < lax.broadcasted_iota(
            jnp.int32, (rows, rows), 1
        )
        before = jnp.dot(named, earlier.astype(F32).astype(BF16), preferred_element_type=F32)
        slot = lax.broadcasted_iota(jnp.int32, (slots, rows), 0)
        pick = None
        for k in range(top):
            place = jnp.sum(jnp.where(here[k], before, 0.0), axis=0, keepdims=True).astype(jnp.int32)
            dest = ids_ref[k : k + 1, :] * room + place
            dest_ref[k : k + 1, :] = dest
            hit = (slot == dest).astype(F32)
            pick = hit if pick is None else pick + hit
        out[...] = jnp.dot(pick.astype(BF16), own, preferred_element_type=F32).astype(BF16)

    return pl.pallas_call(
        kernel,
        out_shape=[jax.ShapeDtypeStruct((slots, cols), BF16), jax.ShapeDtypeStruct((top, rows), jnp.int32)],
        in_specs=[SMEM, VMEM, VMEM, VMEM],
        out_specs=[VMEM, VMEM],
        compiler_params=params(12),
        name="dispatch",
    )(tp_at, tokens, ids, gain)


def fan_out(arrived, copies):
    nz, nc, room, cols = arrived.shape

    def kernel(x, out):
        for c in range(nc):
            block = x[:, c].reshape(nz * room, cols)
            for j in range(copies):
                out[c * copies + j] = block

    return pl.pallas_call(
        kernel,
        out_shape=jax.ShapeDtypeStruct((nc * copies, nz * room, cols), BF16),
        in_specs=[VMEM],
        out_specs=VMEM,
        compiler_params=params(4),
        name="fan_out",
    )(arrived)


def partial_products(x_at, pieces, weights, groups_in, groups_out):
    nx = len(weights)
    blocks, some, cols = pieces.shape
    depth, wide = weights[0].shape
    rows, ny = some * groups_in, blocks // groups_in
    share = rows // groups_out

    def kernel(at, x, *refs):
        w, out, joined = refs[:nx], refs[nx], refs[nx + 1]
        for g in range(groups_in):
            for j in range(ny):
                joined[g * some : (g + 1) * some, j * cols : (j + 1) * cols] = x[g * ny + j]
        for s in range(nx):
            place = lax.rem(at[0] + (nx - s), nx)
            product = jnp.dot(joined[...], w[s][...], preferred_element_type=F32).astype(BF16)
            for g in range(groups_out):
                out[g * nx + place] = product[g * share : (g + 1) * share]

    return pl.pallas_call(
        kernel,
        out_shape=jax.ShapeDtypeStruct((groups_out * nx, share, wide), BF16),
        in_specs=[SMEM, VMEM] + [VMEM] * nx,
        out_specs=VMEM,
        scratch_shapes=[pltpu.VMEM((rows, depth), BF16)],
        compiler_params=params(16),
        cost_estimate=pl.CostEstimate(flops=2 * nx * rows * depth * wide, bytes_accessed=4 << 20, transcendentals=0),
        name="partial_products",
    )(x_at, pieces, *weights)


def hidden_units(parts, copies):
    nx, rows, wide = parts.shape
    ff = wide // 2

    def kernel(p, out):
        total = p[0].astype(F32)
        for j in range(1, nx):
            total += p[j].astype(F32)
        gate = jnp.minimum(total[:, :ff], LIMIT)
        up_part = jnp.clip(total[:, ff:], -LIMIT, LIMIT)
        hidden = ((up_part + 1.0) * gate * jax.nn.sigmoid(ALPHA * gate)).astype(BF16)
        for j in range(copies):
            out[j] = hidden

    return pl.pallas_call(
        kernel,
        out_shape=jax.ShapeDtypeStruct((copies, rows, ff), BF16),
        in_specs=[VMEM],
        out_specs=VMEM,
        compiler_params=params(8),
        name="hidden_units",
    )(parts)


def from_neighbours(blocks, axis):
    n = len(blocks)
    order = dict.fromkeys([1, n - 1] + list(range(2, n - 1)))
    moved = {s: lax.ppermute(blocks[s], axis, shifted(n, s)) for s in order}
    return [blocks[0]] + [moved[s] for s in range(1, n)]


def add_up(parts, groups, blocks):
    total, rows, cols = parts.shape
    terms = total // groups

    def kernel(p, out):
        for g in range(groups):
            value = p[g * terms].astype(F32)
            for j in range(1, terms):
                value += p[g * terms + j].astype(F32)
            out[:, g] = value.astype(BF16).reshape(blocks, rows // blocks, cols)

    return pl.pallas_call(
        kernel,
        out_shape=jax.ShapeDtypeStruct((blocks, groups, rows // blocks, cols), BF16),
        in_specs=[VMEM],
        out_specs=VMEM,
        compiler_params=params(4),
        name="add_up",
    )(parts)


def on_device(tokens, expert_ids, route_weight, norm_gain, gate_weight, up_weight, down_weight):
    nz, nc, ny, nx = (lax.axis_size(a) for a in ("z", "c", "y", "x"))
    x_at, y_at = lax.axis_index("x"), lax.axis_index("y")
    at = x_at.reshape(1).astype(jnp.int32)
    tp_at = (x_at * ny + y_at).reshape(1).astype(jnp.int32)
    rows, width = tokens.shape
    top = expert_ids.shape[1]
    experts = nz * nc * gate_weight.shape[0]
    cap = 5 * rows * top // (4 * experts)
    room = -(-cap // 16) * 16
    slots = experts * room
    cols = width // (nx * ny)
    ff = gate_weight.shape[2]

    buffer, dest = dispatch(tp_at, tokens, expert_ids.T, norm_gain.reshape(1, width), experts, room, cols)
    gate_weight, buffer = lax.optimization_barrier((gate_weight, buffer))
    quarters = weight_quarters(
        at, gate_weight[0], up_weight[0], down_weight.reshape(ny, nx, ff, cols), nx
    )
    pair, down = quarters[:nx], quarters[nx:]

    arrived = swap(buffer.reshape(nz, nc * room, cols), "z").reshape(nz, nc, room, cols)
    pair = from_neighbours(pair, "x")
    blocks = fan_out(arrived, ny)
    pieces = swap(blocks, ("c", "y"))
    down = [d.reshape(ny * ff, cols) for d in from_neighbours(down, "x")]
    parts = partial_products(at, pieces, pair, nc, 1)
    parts = swap(parts, "x")

    hidden = hidden_units(parts, ny)
    pieces = swap(hidden, "y")
    parts = swap(partial_products(at, pieces, down, 1, nc), ("c", "x"))

    back = swap(add_up(parts, nc, nz).reshape(nz, nc * room, cols), "z").reshape(slots, cols)
    slot = jnp.arange(slots, dtype=jnp.int32)
    mixed = 0.0
    for k in range(top):
        chosen = (dest[k][:, None] == slot[None, :]).astype(BF16)
        mixed += jnp.dot(chosen, back, preferred_element_type=F32) * route_weight[:, k, None]
    return mixed.astype(BF16)


def solution(mesh):
    torus = Mesh(mesh.devices.reshape(mesh.shape["ep"] // 2, 2, 8, 4), ("z", "c", "y", "x"))
    ep, tp = ("z", "c"), ("y", "x")
    in_specs = (
        P(ep, None),
        P(ep, None),
        P(ep, None),
        P(),
        P(ep, None, tp),
        P(ep, None, tp),
        P(ep, None, tp),
    )

    return jax.shard_map(on_device, mesh=torus, in_specs=in_specs, out_specs=P(ep, tp), check_vma=False)
```

profile of v0, /device:TPU:2, one launch (start us, length us, event | category | flops | bytes accessed | tf_op | source)
XLA Modules:
  0.0 171.1 jit_solution(5690411300872326569)
XLA Ops:
  0.0 1.4 copy-done
  1.4 0.7 copy-done.6
  2.1 0.7 copy-done.7
  2.8 0.7 dispatch.1
  3.5 33.5 %all_to_all.30 = bf16[16,32,128]{2,1,0:T(8,128)(2,1)S(1)} all-to-all(bf16[16,32,128]{2,1,0:T(8,128)(2,1)S(1)} %bitcast.29), channel_id=1, replica_groups=mesh['z'=16,'c'=2,'y'=8,'x'=4] {'z'}, dimensions={0} | all-to-all | bytes 262144 | tf_op jit(solution)/shard_map/all_to_all | solution.py:26
  36.9 1.1 fan_out.1
  38.0 7.2 %all-to-all-start.1 = ((bf16[16,256,128]{2,1,0:T(8,128)(2,1)}), bf16[16,256,128]{2,1,0:T(8,128)(2,1)S(1)}, u32[]{:S(2)}, u32[]{:S(2)}) async-start(bf16[16,256,128]{2,1,0:T(8,128)(2,1)} %fan_out.1), calls=%async_computation.1 | async-start | bytes 2097152 | tf_op jit(solution)/shard_map/all_to_all | solution.py:26
  45.3 0.0 copy-done.1
  45.3 0.0 copy-done.2
  45.3 0.0 copy-start.3
  45.3 1.2 copy-done.3
  46.5 0.6 weight_quarters.1
  47.1 0.0 copy-start.4
  47.1 0.8 copy-done.4
  47.9 0.7 copy-done.8
  48.6 0.7 copy-done.10
  49.3 0.7 copy-done.12
  50.0 3.4 %collective-permute-start = (bf16[1024,256]{1,0:T(8,128)(2,1)S(1)}, bf16[1024,256]{1,0:T(8,128)(2,1)S(1)}, u32[]{:S(2)}, u32[]{:S(2)}) collective-permute-start(bf16[1024,256]{1,0:T(8,128)(2,1)S(1)} %get-tuple-element.22), channel_id=1, source_target_pairs={{0,1},{1,2},{2,3},{3,0},{4,5},{5,6},{6,7},{7,4},{8,9},{9,10},{10,1... | collective-permute-start | bytes 1572872 | tf_op jit(solution)/shard_map/ppermute | solution.py:182
  53.4 3.0 %collective-permute-start.1 = (bf16[1024,256]{1,0:T(8,128)(2,1)S(1)}, bf16[1024,256]{1,0:T(8,128)(2,1)S(1)}, u32[]{:S(2)}, u32[]{:S(2)}) collective-permute-start(bf16[1024,256]{1,0:T(8,128)(2,1)S(1)} %get-tuple-element.23), channel_id=1, source_target_pairs={{0,2},{1,3},{2,0},{3,1},{4,6},{5,7},{6,4},{7,5},{8,10},{9,11},{10,... | collective-permute-start | bytes 1572872 | tf_op jit(solution)/shard_map/ppermute | solution.py:182
  56.5 4.1 %collective-permute-start.2 = (bf16[1024,256]{1,0:T(8,128)(2,1)S(1)}, bf16[1024,256]{1,0:T(8,128)(2,1)S(1)}, u32[]{:S(2)}, u32[]{:S(2)}) collective-permute-start(bf16[1024,256]{1,0:T(8,128)(2,1)S(1)} %get-tuple-element.24), channel_id=1, source_target_pairs={{0,3},{1,0},{2,1},{3,2},{4,7},{5,4},{6,5},{7,6},{8,11},{9,8},{10,9... | collective-permute-start | bytes 1572872 | tf_op jit(solution)/shard_map/ppermute | solution.py:182
  60.5 6.2 %collective-permute-done.refs_1_ = bf16[1024,256]{1,0:T(8,128)(2,1)S(1)} collective-permute-done((bf16[1024,256]{1,0:T(8,128)(2,1)S(1)}, bf16[1024,256]{1,0:T(8,128)(2,1)S(1)}, u32[]{:S(2)}, u32[]{:S(2)}) %collective-permute-start) | collective-permute-done | bytes 524320 | tf_op jit(solution)/shard_map/ppermute | solution.py:182
  66.7 5.0 %collective-permute-done.1.refs_2_ = bf16[1024,256]{1,0:T(8,128)(2,1)S(1)} collective-permute-done((bf16[1024,256]{1,0:T(8,128)(2,1)S(1)}, bf16[1024,256]{1,0:T(8,128)(2,1)S(1)}, u32[]{:S(2)}, u32[]{:S(2)}) %collective-permute-start.1) | collective-permute-done | bytes 524320 | tf_op jit(solution)/shard_map/ppermute | solution.py:182
  71.7 10.4 %collective-permute-done.2.refs_3_ = bf16[1024,256]{1,0:T(8,128)(2,1)S(1)} collective-permute-done((bf16[1024,256]{1,0:T(8,128)(2,1)S(1)}, bf16[1024,256]{1,0:T(8,128)(2,1)S(1)}, u32[]{:S(2)}, u32[]{:S(2)}) %collective-permute-start.2) | collective-permute-done | bytes 524320 | tf_op jit(solution)/shard_map/ppermute | solution.py:182
  82.0 0.0 all-to-all-done.1.x
  82.0 1.0 copy-done.5
  83.1 1.3 partial_products.2
  84.4 17.2 %all_to_all.31.p = bf16[4,512,256]{2,1,0:T(8,128)(2,1)S(1)} all-to-all(bf16[4,512,256]{2,1,0:T(8,128)(2,1)S(1)} %partial_products.2), channel_id=1, replica_groups=mesh['z'=16,'c'=2,'y'=8,'x'=4] {'x'}, dimensions={0} | all-to-all | bytes 2097152 | tf_op jit(solution)/shard_map/all_to_all | solution.py:26
  101.5 1.2 hidden_units.1
  102.7 6.9 %all-to-all-start.3 = ((bf16[8,512,128]{2,1,0:T(8,128)(2,1)}), bf16[8,512,128]{2,1,0:T(8,128)(2,1)S(1)}, u32[]{:S(2)}, u32[]{:S(2)}) async-start(bf16[8,512,128]{2,1,0:T(8,128)(2,1)} %hidden_units.1), calls=%async_computation.3 | async-start | bytes 2097152 | tf_op jit(solution)/shard_map/all_to_all | solution.py:26
  109.7 0.0 copy-done.13
  109.7 2.1 %collective-permute-start.3 = (bf16[8,128,128]{2,1,0:T(8,128)(2,1)S(1)}, bf16[8,128,128]{2,1,0:T(8,128)(2,1)S(1)}, u32[]{:S(2)}, u32[]{:S(2)}) collective-permute-start(bf16[8,128,128]{2,1,0:T(8,128)(2,1)S(1)} %copy-done.13), channel_id=1, source_target_pairs={{0,1},{1,2},{2,3},{3,0},{4,5},{5,6},{6,7},{7,4},{8,9},{9,10},{10,1... | collective-permute-start | bytes 786440 | tf_op jit(solution)/shard_map/ppermute | solution.py:182
  111.8 0.0 copy-done.11
  111.8 5.2 %collective-permute-start.4 = (bf16[8,128,128]{2,1,0:T(8,128)(2,1)S(1)}, bf16[8,128,128]{2,1,0:T(8,128)(2,1)S(1)}, u32[]{:S(2)}, u32[]{:S(2)}) collective-permute-start(bf16[8,128,128]{2,1,0:T(8,128)(2,1)S(1)} %copy-done.11), channel_id=1, source_target_pairs={{0,2},{1,3},{2,0},{3,1},{4,6},{5,7},{6,4},{7,5},{8,10},{9,11},{10,... | collective-permute-start | bytes 786440 | tf_op jit(solution)/shard_map/ppermute | solution.py:182
  117.0 0.0 copy-done.9
  117.0 2.5 %collective-permute-start.5 = (bf16[8,128,128]{2,1,0:T(8,128)(2,1)S(1)}, bf16[8,128,128]{2,1,0:T(8,128)(2,1)S(1)}, u32[]{:S(2)}, u32[]{:S(2)}) collective-permute-start(bf16[8,128,128]{2,1,0:T(8,128)(2,1)S(1)} %copy-done.9), channel_id=1, source_target_pairs={{0,3},{1,0},{2,1},{3,2},{4,7},{5,4},{6,5},{7,6},{8,11},{9,8},{10,9... | collective-permute-start | bytes 786440 | tf_op jit(solution)/shard_map/ppermute | solution.py:182
  119.5 0.3 collective-permute-done.3
  119.9 4.5 %collective-permute-done.4 = bf16[8,128,128]{2,1,0:T(8,128)(2,1)S(1)} collective-permute-done((bf16[8,128,128]{2,1,0:T(8,128)(2,1)S(1)}, bf16[8,128,128]{2,1,0:T(8,128)(2,1)S(1)}, u32[]{:S(2)}, u32[]{:S(2)}) %collective-permute-start.4) | collective-permute-done | bytes 262176 | tf_op jit(solution)/shard_map/ppermute | solution.py:182
  124.3 3.1 %collective-permute-done.5 = bf16[8,128,128]{2,1,0:T(8,128)(2,1)S(1)} collective-permute-done((bf16[8,128,128]{2,1,0:T(8,128)(2,1)S(1)}, bf16[8,128,128]{2,1,0:T(8,128)(2,1)S(1)}, u32[]{:S(2)}, u32[]{:S(2)}) %collective-permute-start.5) | collective-permute-done | bytes 262176 | tf_op jit(solution)/shard_map/ppermute | solution.py:182
  127.4 9.6 %all-to-all-done.3.x = bf16[8,512,128]{2,1,0:T(8,128)(2,1)S(1)} async-done(((bf16[8,512,128]{2,1,0:T(8,128)(2,1)}), bf16[8,512,128]{2,1,0:T(8,128)(2,1)S(1)}, u32[]{:S(2)}, u32[]{:S(2)}) %all-to-all-start.3) | async-done | bytes 1048608 | tf_op jit(solution)/shard_map/all_to_all | solution.py:26
  137.0 1.3 partial_products.3
  138.3 0.0 copy-start.14
  138.3 12.4 %all_to_all.32.p = bf16[8,256,128]{2,1,0:T(8,128)(2,1)S(1)} all-to-all(bf16[8,256,128]{2,1,0:T(8,128)(2,1)S(1)} %partial_products.3), channel_id=1, replica_groups=mesh['z'=16,'c'=2,'y'=8,'x'=4] {'c','x'}, dimensions={0} | all-to-all | bytes 1048576 | tf_op jit(solution)/shard_map/all_to_all | solution.py:26
  150.7 0.7 add_up.1
  151.4 3.8 %all-to-all-start.5 = ((bf16[16,32,128]{2,1,0:T(8,128)(2,1)}), bf16[16,32,128]{2,1,0:T(8,128)(2,1)S(1)}, u32[]{:S(2)}, u32[]{:S(2)}) async-start(bf16[16,32,128]{2,1,0:T(8,128)(2,1)} %bitcast.14), calls=%async_computation.5 | async-start | bytes 262144 | tf_op jit(solution)/shard_map/all_to_all | solution.py:26
  155.2 0.0 copy-done.14
  155.2 14.7 %all-to-all-done.5 = bf16[16,32,128]{2,1,0:T(8,128)(2,1)S(1)} async-done(((bf16[16,32,128]{2,1,0:T(8,128)(2,1)}), bf16[16,32,128]{2,1,0:T(8,128)(2,1)S(1)}, u32[]{:S(2)}, u32[]{:S(2)}) %all-to-all-start.5) | async-done | bytes 131104 | tf_op jit(solution)/shard_map/all_to_all | solution.py:26
  170.0 0.3 convolution_multiply_fusion
  170.2 0.9 fusion.1
  (14 shorter events, 0.0 us)
Async XLA Ops:
  0.0 1.4 copy-start
  1.4 0.7 copy-start.6
  2.1 0.7 copy-start.7
  36.9 8.3 %copy-start.1 = (bf16[1,4096,128]{2,1,0:T(8,128)(2,1)S(1)}, bf16[1,4096,128]{2,1,0:T(8,128)(2,1)}, u32[]{:S(2)}) copy-start(bf16[1,4096,128]{2,1,0:T(8,128)(2,1)} %param.11) | copy-start | bytes 3145732
  36.9 8.4 %copy-start.2 = (bf16[1,4096,128]{2,1,0:T(8,128)(2,1)S(1)}, bf16[1,4096,128]{2,1,0:T(8,128)(2,1)}, u32[]{:S(2)}) copy-start(bf16[1,4096,128]{2,1,0:T(8,128)(2,1)} %param.12) | copy-start | bytes 3145732
  38.0 44.0 %all-to-all-start.1 = ((bf16[16,256,128]{2,1,0:T(8,128)(2,1)}), bf16[16,256,128]{2,1,0:T(8,128)(2,1)S(1)}, u32[]{:S(2)}, u32[]{:S(2)}) async-start(bf16[16,256,128]{2,1,0:T(8,128)(2,1)} %fan_out.1), calls=%async_computation.1 | async-start | bytes 2097152 | tf_op jit(solution)/shard_map/all_to_all | solution.py:26
  45.3 1.2 copy-start.3
  47.1 0.8 copy-start.4
  47.9 0.7 copy-start.8
  48.6 0.7 copy-start.10
  49.3 0.7 copy-start.12
  50.0 16.7 %collective-permute-start = (bf16[1024,256]{1,0:T(8,128)(2,1)S(1)}, bf16[1024,256]{1,0:T(8,128)(2,1)S(1)}, u32[]{:S(2)}, u32[]{:S(2)}) collective-permute-start(bf16[1024,256]{1,0:T(8,128)(2,1)S(1)} %get-tuple-element.22), channel_id=1, source_target_pairs={{0,1},{1,2},{2,3},{3,0},{4,5},{5,6},{6,7},{7,4},{8,9},{9,10},{10,1... | collective-permute-start | bytes 1572872 | tf_op jit(solution)/shard_map/ppermute | solution.py:182
  53.4 18.2 %collective-permute-start.1 = (bf16[1024,256]{1,0:T(8,128)(2,1)S(1)}, bf16[1024,256]{1,0:T(8,128)(2,1)S(1)}, u32[]{:S(2)}, u32[]{:S(2)}) collective-permute-start(bf16[1024,256]{1,0:T(8,128)(2,1)S(1)} %get-tuple-element.23), channel_id=1, source_target_pairs={{0,2},{1,3},{2,0},{3,1},{4,6},{5,7},{6,4},{7,5},{8,10},{9,11},{10,... | collective-permute-start | bytes 1572872 | tf_op jit(solution)/shard_map/ppermute | solution.py:182
  56.5 25.6 %collective-permute-start.2 = (bf16[1024,256]{1,0:T(8,128)(2,1)S(1)}, bf16[1024,256]{1,0:T(8,128)(2,1)S(1)}, u32[]{:S(2)}, u32[]{:S(2)}) collective-permute-start(bf16[1024,256]{1,0:T(8,128)(2,1)S(1)} %get-tuple-element.24), channel_id=1, source_target_pairs={{0,3},{1,0},{2,1},{3,2},{4,7},{5,4},{6,5},{7,6},{8,11},{9,8},{10,9... | collective-permute-start | bytes 1572872 | tf_op jit(solution)/shard_map/ppermute | solution.py:182
  82.0 1.0 copy-start.5
  102.7 7.0 %copy-start.13 = (bf16[8,128,128]{2,1,0:T(8,128)(2,1)S(1)}, bf16[8,128,128]{2,1,0:T(8,128)(2,1)}, u32[]{:S(2)}) copy-start(bf16[8,128,128]{2,1,0:T(8,128)(2,1)} %copy-done.12) | copy-start | bytes 786436
  102.7 9.1 %copy-start.11 = (bf16[8,128,128]{2,1,0:T(8,128)(2,1)S(1)}, bf16[8,128,128]{2,1,0:T(8,128)(2,1)}, u32[]{:S(2)}) copy-start(bf16[8,128,128]{2,1,0:T(8,128)(2,1)} %copy-done.10) | copy-start | bytes 786436
  102.7 14.3 %copy-start.9 = (bf16[8,128,128]{2,1,0:T(8,128)(2,1)S(1)}, bf16[8,128,128]{2,1,0:T(8,128)(2,1)}, u32[]{:S(2)}) copy-start(bf16[8,128,128]{2,1,0:T(8,128)(2,1)} %copy-done.8) | copy-start | bytes 786436
  102.7 34.3 %all-to-all-start.3 = ((bf16[8,512,128]{2,1,0:T(8,128)(2,1)}), bf16[8,512,128]{2,1,0:T(8,128)(2,1)S(1)}, u32[]{:S(2)}, u32[]{:S(2)}) async-start(bf16[8,512,128]{2,1,0:T(8,128)(2,1)} %hidden_units.1), calls=%async_computation.3 | async-start | bytes 2097152 | tf_op jit(solution)/shard_map/all_to_all | solution.py:26
  109.7 10.2 %collective-permute-start.3 = (bf16[8,128,128]{2,1,0:T(8,128)(2,1)S(1)}, bf16[8,128,128]{2,1,0:T(8,128)(2,1)S(1)}, u32[]{:S(2)}, u32[]{:S(2)}) collective-permute-start(bf16[8,128,128]{2,1,0:T(8,128)(2,1)S(1)} %copy-done.13), channel_id=1, source_target_pairs={{0,1},{1,2},{2,3},{3,0},{4,5},{5,6},{6,7},{7,4},{8,9},{9,10},{10,1... | collective-permute-start | bytes 786440 | tf_op jit(solution)/shard_map/ppermute | solution.py:182
  111.8 12.5 %collective-permute-start.4 = (bf16[8,128,128]{2,1,0:T(8,128)(2,1)S(1)}, bf16[8,128,128]{2,1,0:T(8,128)(2,1)S(1)}, u32[]{:S(2)}, u32[]{:S(2)}) collective-permute-start(bf16[8,128,128]{2,1,0:T(8,128)(2,1)S(1)} %copy-done.11), channel_id=1, source_target_pairs={{0,2},{1,3},{2,0},{3,1},{4,6},{5,7},{6,4},{7,5},{8,10},{9,11},{10,... | collective-permute-start | bytes 786440 | tf_op jit(solution)/shard_map/ppermute | solution.py:182
  117.0 10.4 %collective-permute-start.5 = (bf16[8,128,128]{2,1,0:T(8,128)(2,1)S(1)}, bf16[8,128,128]{2,1,0:T(8,128)(2,1)S(1)}, u32[]{:S(2)}, u32[]{:S(2)}) collective-permute-start(bf16[8,128,128]{2,1,0:T(8,128)(2,1)S(1)} %copy-done.9), channel_id=1, source_target_pairs={{0,3},{1,0},{2,1},{3,2},{4,7},{5,4},{6,5},{7,6},{8,11},{9,8},{10,9... | collective-permute-start | bytes 786440 | tf_op jit(solution)/shard_map/ppermute | solution.py:182
  138.3 16.9 %copy-start.14 = (f32[192,2]{0,1:T(2,128)S(1)}, f32[192,2]{0,1:T(2,128)}, u32[]{:S(2)}) copy-start(f32[192,2]{0,1:T(2,128)} %param.9) | copy-start | bytes 4612
  151.4 18.5 %all-to-all-start.5 = ((bf16[16,32,128]{2,1,0:T(8,128)(2,1)}), bf16[16,32,128]{2,1,0:T(8,128)(2,1)S(1)}, u32[]{:S(2)}, u32[]{:S(2)}) async-start(bf16[16,32,128]{2,1,0:T(8,128)(2,1)} %bitcast.14), calls=%async_computation.5 | async-start | bytes 262144 | tf_op jit(solution)/shard_map/all_to_all | solution.py:26
where the time goes:
time: 172 us; the launch traced here: 171 us
  blocking collectives  63 us (37%)
  waiting for transfers between devices  53.7 us (31%)
  starting transfers between devices  38.2 us (22%)
  local copies, waits for them, and re-layouts  8.05 us (5%)
  Pallas kernels  6.79 us (4%)
    all_to_all x3, blocking collectives, swap(): return lax.all_to_all(x, axes, split_axis=0, concat_axis=0, tiled=True)  63 us
    ppermute x6, waiting for transfers between devices, from_neighbours(): moved = {s: lax.ppermute(blocks[s], axis, shifted(n, s)) for s in order}  29.4 us
    all_to_all x3, waiting for transfers between devices, swap(): return lax.all_to_all(x, axes, split_axis=0, concat_axis=0, tiled=True)  24.4 us
    ppermute x6, starting transfers between devices, from_neighbours(): moved = {s: lax.ppermute(blocks[s], axis, shifted(n, s)) for s in order}  20.3 us
    all_to_all x3, starting transfers between devices, swap(): return lax.all_to_all(x, axes, split_axis=0, concat_axis=0, tiled=True)  17.9 us
    unnamed x30, local copies, waits for them, and re-layouts  8.04 us
  transfers between devices with their start and end apart: 9, of which 8 were waited for; matrix products, arithmetic and copies ran while one was open for 0% of the time, Pallas kernels for 0%

commit v1 on v0

--- a/solution.py
+++ b/solution.py
@@ -34,9 +34,10 @@
     width, ff = gate_weight.shape
     ny, _, _, cols = down_weight.shape
     rows = width // nx
+    each = 2 + ny
 
     def kernel(at, gate, up, down, *refs):
-        outs, sem = refs[: 2 * nx], refs[2 * nx]
+        outs, sem = refs[:nx], refs[nx]
         copies = []
         for s in range(nx):
             quarter = lax.rem(at[0] + s, nx)
@@ -45,10 +46,17 @@
                     pltpu.make_async_copy(
                         src.at[pl.ds(quarter * rows, rows)],
                         outs[s].at[:, pl.ds(side * ff, ff)],
-                        sem.at[3 * s + side],
+                        sem.at[each * s + side],
                     )
                 )
-            copies.append(pltpu.make_async_copy(down.at[:, quarter], outs[nx + s], sem.at[3 * s + 2]))
+            for j in range(ny):
+                copies.append(
+                    pltpu.make_async_copy(
+                        down.at[j, quarter],
+                        outs[s].at[pl.ds(j * ff, ff), pl.ds(2 * ff, cols)],
+                        sem.at[each * s + 2 + j],
+                    )
+                )
         for copy in copies:
             copy.start()
         for copy in copies:
@@ -56,12 +64,11 @@
 
     return pl.pallas_call(
         kernel,
-        out_shape=[jax.ShapeDtypeStruct((rows, 2 * ff), BF16)] * nx
-        + [jax.ShapeDtypeStruct((ny, ff, cols), BF16)] * nx,
+        out_shape=[jax.ShapeDtypeStruct((rows, 2 * ff + cols), BF16)] * nx,
         in_specs=[SMEM, HBM, HBM, HBM],
-        out_specs=[VMEM] * (2 * nx),
-        scratch_shapes=[pltpu.SemaphoreType.DMA((3 * nx,))],
-        compiler_params=params(4),
+        out_specs=[HBM] * nx,
+        scratch_shapes=[pltpu.SemaphoreType.DMA((each * nx,))],
+        compiler_params=params(2),
         name="weight_quarters",
     )(x_at, gate_weight, up_weight, down_weight)
 
@@ -70,12 +77,23 @@
     rows, width = tokens.shape
     top = ids.shape[0]
     slots = experts * room
-
-    def kernel(at, tok, ids_ref, gain_ref, out, dest_ref):
-        values = tok[...].astype(F32)
-        scale = lax.rsqrt(jnp.sum(values * values, axis=-1, keepdims=True) * (1.0 / width) + EPS)
+    chunks = 4 if rows % 64 == 0 else 1
+    step = rows // chunks
+
+    def kernel(at, tok_hbm, ids_hbm, gain_hbm, out, dest_ref, tok, ids_ref, gain_ref, own_ref, sem):
         start = pl.multiple_of(at[0] * cols, cols)
-        own = (tok[:, pl.ds(start, cols)].astype(F32) * scale * gain_ref[:, pl.ds(start, cols)]).astype(BF16)
+        small = [
+            pltpu.make_async_copy(ids_hbm, ids_ref, sem.at[chunks]),
+            pltpu.make_async_copy(gain_hbm.at[:, pl.ds(start, cols)], gain_ref, sem.at[chunks + 1]),
+        ]
+        large = [
+            pltpu.make_async_copy(tok_hbm.at[pl.ds(i * step, step)], tok.at[pl.ds(i * step, step)], sem.at[i])
+            for i in range(chunks)
+        ]
+        for copy in small + large:
+            copy.start()
+        for copy in small:
+            copy.wait()
         expert = lax.broadcasted_iota(jnp.int32, (experts, rows), 0)
         here = [ids_ref[k : k + 1, :] == expert for k in range(top)]
         named = sum(h.astype(F32) for h in here).astype(BF16)
@@ -91,13 +109,28 @@
             dest_ref[k : k + 1, :] = dest
             hit = (slot == dest).astype(F32)
             pick = hit if pick is None else pick + hit
-        out[...] = jnp.dot(pick.astype(BF16), own, preferred_element_type=F32).astype(BF16)
+        pick = pick.astype(BF16)
+        for i in range(chunks):
+            large[i].wait()
+            at_rows = slice(i * step, (i + 1) * step)
+            values = tok[at_rows, :].astype(F32)
+            scale = lax.rsqrt(jnp.sum(values * values, axis=-1, keepdims=True) * (1.0 / width) + EPS)
+            own = tok[at_rows, pl.ds(start, cols)].astype(F32)
+            own_ref[at_rows, :] = (own * scale * gain_ref[...]).astype(BF16)
+        out[...] = jnp.dot(pick, own_ref[...], preferred_element_type=F32).astype(BF16)
 
     return pl.pallas_call(
         kernel,
         out_shape=[jax.ShapeDtypeStruct((slots, cols), BF16), jax.ShapeDtypeStruct((top, rows), jnp.int32)],
-        in_specs=[SMEM, VMEM, VMEM, VMEM],
+        in_specs=[SMEM, HBM, HBM, HBM],
         out_specs=[VMEM, VMEM],
+        scratch_shapes=[
+            pltpu.VMEM((rows, width), BF16),
+            pltpu.VMEM((top, rows), jnp.int32),
+            pltpu.VMEM((1, cols), F32),
+            pltpu.VMEM((rows, cols), BF16),
+            pltpu.SemaphoreType.DMA((chunks + 2,)),
+        ],
         compiler_params=params(12),
         name="dispatch",
     )(tp_at, tokens, ids, gain)
@@ -122,34 +155,51 @@
     )(arrived)
 
 
-def partial_products(x_at, pieces, weights, groups_in, groups_out):
+def join(pieces, groups):
+    blocks, some, cols = pieces.shape
+    rows, ny = some * groups, blocks // groups
+
+    def kernel(x, out):
+        for g in range(groups):
+            for j in range(ny):
+                out[g * some : (g + 1) * some, j * cols : (j + 1) * cols] = x[g * ny + j]
+
+    return pl.pallas_call(
+        kernel,
+        out_shape=jax.ShapeDtypeStruct((rows, ny * cols), BF16),
+        in_specs=[VMEM],
+        out_specs=VMEM,
+        compiler_params=params(4),
+        name="join",
+    )(pieces)
+
+
+def partial_products(x_at, left, weights, first, wide, groups):
     nx = len(weights)
-    blocks, some, cols = pieces.shape
-    depth, wide = weights[0].shape
-    rows, ny = some * groups_in, blocks // groups_in
-    share = rows // groups_out
+    rows, depth = left.shape
+    share = rows // groups
+    pairs = 256 // wide
 
     def kernel(at, x, *refs):
-        w, out, joined = refs[:nx], refs[nx], refs[nx + 1]
-        for g in range(groups_in):
-            for j in range(ny):
-                joined[g * some : (g + 1) * some, j * cols : (j + 1) * cols] = x[g * ny + j]
-        for s in range(nx):
-            place = lax.rem(at[0] + (nx - s), nx)
-            product = jnp.dot(joined[...], w[s][...], preferred_element_type=F32).astype(BF16)
-            for g in range(groups_out):
-                out[g * nx + place] = product[g * share : (g + 1) * share]
-
-    return pl.pallas_call(
-        kernel,
-        out_shape=jax.ShapeDtypeStruct((groups_out * nx, share, wide), BF16),
+        w, out = refs[:nx], refs[nx]
+        for s in range(0, nx, pairs):
+            right = [w[s + i][:, first : first + wide] for i in range(pairs)]
+            right = right[0] if pairs == 1 else jnp.concatenate(right, axis=1)
+            product = jnp.dot(x[...], right, preferred_element_type=F32).astype(BF16)
+            for i in range(pairs):
+                place = lax.rem(at[0] + (nx - s - i), nx)
+                for g in range(groups):
+                    out[g * nx + place] = product[g * share : (g + 1) * share, i * wide : (i + 1) * wide]
+
+    return pl.pallas_call(
+        kernel,
+        out_shape=jax.ShapeDtypeStruct((groups * nx, share, wide), BF16),
         in_specs=[SMEM, VMEM] + [VMEM] * nx,
         out_specs=VMEM,
-        scratch_shapes=[pltpu.VMEM((rows, depth), BF16)],
         compiler_params=params(16),
         cost_estimate=pl.CostEstimate(flops=2 * nx * rows * depth * wide, bytes_accessed=4 << 20, transcendentals=0),
         name="partial_products",
-    )(x_at, pieces, *weights)
+    )(x_at, left, *weights)
 
 
 def hidden_units(parts, copies):
@@ -202,6 +252,30 @@
         compiler_params=params(4),
         name="add_up",
     )(parts)
+
+
+def combine(back, dest, route):
+    slots, cols = back.shape
+    top, rows = dest.shape
+
+    def kernel(x, dest_ref, route_ref, out):
+        slot = lax.broadcasted_iota(jnp.int32, (slots, rows), 0)
+        total = None
+        for k in range(top):
+            chosen = (slot == dest_ref[k : k + 1, :]).astype(F32).astype(BF16)
+            copy = lax.dot_general(chosen, x[...], (((0,), (0,)), ((), ())), preferred_element_type=F32)
+            copy = copy * route_ref[k]
+            total = copy if total is None else total + copy
+        out[...] = total.astype(BF16)
+
+    return pl.pallas_call(
+        kernel,
+        out_shape=jax.ShapeDtypeStruct((rows, cols), BF16),
+        in_specs=[VMEM, VMEM, VMEM],
+        out_specs=VMEM,
+        compiler_params=params(8),
+        name="combine",
+    )(back, dest, route)
 
 
 def on_device(tokens, expert_ids, route_weight, norm_gain, gate_weight, up_weight, down_weight):
@@ -220,30 +294,26 @@
 
     buffer, dest = dispatch(tp_at, tokens, expert_ids.T, norm_gain.reshape(1, width), experts, room, cols)
     gate_weight, buffer = lax.optimization_barrier((gate_weight, buffer))
-    quarters = weight_quarters(
+    weights = weight_quarters(
         at, gate_weight[0], up_weight[0], down_weight.reshape(ny, nx, ff, cols), nx
     )
-    pair, down = quarters[:nx], quarters[nx:]
 
     arrived = swap(buffer.reshape(nz, nc * room, cols), "z").reshape(nz, nc, room, cols)
-    pair = from_neighbours(pair, "x")
+    weights = from_neighbours(weights, "x")
     blocks = fan_out(arrived, ny)
     pieces = swap(blocks, ("c", "y"))
-    down = [d.reshape(ny * ff, cols) for d in from_neighbours(down, "x")]
-    parts = partial_products(at, pieces, pair, nc, 1)
+    left = join(pieces, nc)
+    parts = partial_products(at, left, weights, 0, 2 * ff, 1)
     parts = swap(parts, "x")
 
     hidden = hidden_units(parts, ny)
     pieces = swap(hidden, "y")
-    parts = swap(partial_products(at, pieces, down, 1, nc), ("c", "x"))
-
-    back = swap(add_up(parts, nc, nz).reshape(nz, nc * room, cols), "z").reshape(slots, cols)
-    slot = jnp.arange(slots, dtype=jnp.int32)
-    mixed = 0.0
-    for k in range(top):
-        chosen = (dest[k][:, None] == slot[None, :]).astype(BF16)
-        mixed += jnp.dot(chosen, back, preferred_element_type=F32) * route_weight[:, k, None]
-    return mixed.astype(BF16)
+    parts = partial_products(at, join(pieces, 1), weights, 2 * ff, cols, nc)
+    parts = swap(parts, ("c", "x"))
+
+    result = add_up(parts, nc, nz).reshape(nz, nc * room, cols)
+    back = swap(result, "z").reshape(slots, cols)
+    return combine(back, dest, jnp.broadcast_to(route_weight.T[:, :, None], (top, rows, cols)))
 
 
 def solution(mesh):

time: 172 us -> 183 us (1.064)
  blocking collectives: 63 us -> 115 us
  waiting for transfers between devices: 53.7 us -> 32.8 us
  starting transfers between devices: 38.2 us -> 17.7 us
  Pallas kernels: 6.79 us -> 11.1 us
  local copies, waits for them, and re-layouts: 8.05 us -> 5.36 us
    all_to_all x3 -> x5, blocking collectives: 63 us -> 115 us  [swap(): return lax.all_to_all(x, axes, split_axis=0, concat_axis=0, tiled=True)]
    all_to_all x3 -> x1, waiting for transfers between devices: 24.4 us -> 10.7 us  [swap(): return lax.all_to_all(x, axes, split_axis=0, concat_axis=0, tiled=True)]
    all_to_all x3 -> x1, starting transfers between devices: 17.9 us -> 7.2 us  [swap(): return lax.all_to_all(x, axes, split_axis=0, concat_axis=0, tiled=True)]
    ppermute x6 -> x3, starting transfers between devices: 20.3 us -> 10.5 us  [from_neighbours(): moved = {s: lax.ppermute(blocks[s], axis, shifted(n, s)) for s in order}]
    ppermute x6 -> x3, waiting for transfers between devices: 29.4 us -> 22.1 us  [from_neighbours(): moved = {s: lax.ppermute(blocks[s], axis, shifted(n, s)) for s in order}]
    pallas_call x3 -> x6, Pallas kernels: 3.11 us -> 7.67 us  [the longest x2 4.23 us: partial_products(): pl.pallas_call(kernel, out_shape=jax.ShapeDtypeStruct((groups * nx, share...]
    unnamed x30 -> x14, local copies, waits for them, and re-layouts: 8.04 us -> 5.26 us
  transfers between devices with their start and end apart: 9 -> 4, of which waited for: 8 -> 4; matrix products, arithmetic and copies ran while one was open for 0% -> 0% of each run, Pallas kernels for 0% -> 1%
where the time goes in v1:
time: 183 us; the launch traced here: 182 us
  blocking collectives  115 us (63%)
  waiting for transfers between devices  32.8 us (18%)
  starting transfers between devices  17.7 us (10%)
  Pallas kernels  11.1 us (6%)
  local copies, waits for them, and re-layouts  5.36 us (3%)
    all_to_all x5, blocking collectives, swap(): return lax.all_to_all(x, axes, split_axis=0, concat_axis=0, tiled=True)  115 us
    ppermute x3, waiting for transfers between devices, from_neighbours(): moved = {s: lax.ppermute(blocks[s], axis, shifted(n, s)) for s in order}  22.1 us
    all_to_all x1, waiting for transfers between devices, swap(): return lax.all_to_all(x, axes, split_axis=0, concat_axis=0, tiled=True)  10.7 us
    ppermute x3, starting transfers between devices, from_neighbours(): moved = {s: lax.ppermute(blocks[s], axis, shifted(n, s)) for s in order}  10.5 us
    all_to_all x1, starting transfers between devices, swap(): return lax.all_to_all(x, axes, split_axis=0, concat_axis=0, tiled=True)  7.2 us
    unnamed x14, local copies, waits for them, and re-layouts  5.26 us
    pallas_call x2, Pallas kernels, partial_products(): pl.pallas_call(kernel, out_shape=jax.ShapeDtypeStruct((groups * nx, share...  4.23 us
  transfers between devices with their start and end apart: 4, of which 4 were waited for; matrix products, arithmetic and copies ran while one was open for 0% of the time, Pallas kernels for 1%

profile of v1, /device:TPU:2, one launch (start us, length us, event | category | flops | bytes accessed | tf_op | source)
XLA Modules:
  0.0 182.4 jit_solution(3323376712090180826)
XLA Ops:
  0.0 0.0 copy-start
  0.0 1.4 copy-done
  1.4 0.0 copy-start.4
  1.4 0.7 copy-done.4
  2.1 0.0 copy-start.5
  2.1 0.7 copy-done.5
  2.8 2.1 %dispatch.1 = (bf16[512,128]{1,0:T(8,128)(2,1)S(1)}, s32[2,192]{1,0:T(2,128)S(1)}) custom-call(s32[1]{0:T(128)} %bitcast.1.at, bf16[192,4096]{1,0:T(8,128)(2,1)S(1)} %copy-done, s32[2,192]{1,0:T(2,128)S(1)} %bitcast.20, f32[1,4096]{1,0:T(1,128)S(1)} %bitcast.19), custom_call_target="tpu_custom_call" | custom-call | tf_op jit(solution)/shard_map/dispatch/pallas_call | solution.py:122
  4.9 33.5 %all_to_all.30 = bf16[16,32,128]{2,1,0:T(8,128)(2,1)S(1)} all-to-all(bf16[16,32,128]{2,1,0:T(8,128)(2,1)S(1)} %bitcast.18), channel_id=1, replica_groups=mesh['z'=16,'c'=2,'y'=8,'x'=4] {'z'}, dimensions={0} | all-to-all | bytes 262144 | tf_op jit(solution)/shard_map/all_to_all | solution.py:26
  38.4 0.0 copy-start.1
  38.4 1.1 fan_out.1
  39.5 7.2 %all-to-all-start.1 = ((bf16[16,256,128]{2,1,0:T(8,128)(2,1)}), bf16[16,256,128]{2,1,0:T(8,128)(2,1)S(1)}, u32[]{:S(2)}, u32[]{:S(2)}) async-start(bf16[16,256,128]{2,1,0:T(8,128)(2,1)} %fan_out.1), calls=%async_computation.1 | async-start | bytes 2097152 | tf_op jit(solution)/shard_map/all_to_all | solution.py:26
  46.7 0.0 copy-done.1
  46.7 0.0 copy-start.2
  46.7 1.2 copy-done.2
  47.9 0.0 copy-start.3
  47.9 1.2 copy-done.3
  49.2 1.9 %weight_quarters.1 = (bf16[1024,384]{1,0:T(8,128)(2,1)S(1)}, bf16[1024,384]{1,0:T(8,128)(2,1)}, bf16[1024,384]{1,0:T(8,128)(2,1)}, bf16[1024,384]{1,0:T(8,128)(2,1)}) custom-call(s32[1]{0:T(128)} %bitcast.at, bf16[4096,128]{1,0:T(8,128)(2,1)S(1)} %bitcast.12, bf16[4096,128]{1,0:T(8,128)(2,1)S(1)} %bitcast.13, bf16[8,4,128,128]{3,2,1,0:T(8,128)(2,1)S(1)} %bitcast.14), custom_call_target="tpu_custom_call" | custom-call | tf_op jit(solution)/shard_map/weight_quarters/pallas_call | solution.py:65
  51.1 3.4 %collective-permute-start = (bf16[1024,384]{1,0:T(8,128)(2,1)}, bf16[1024,384]{1,0:T(8,128)(2,1)S(1)}, u32[]{:S(2)}, u32[]{:S(2)}) collective-permute-start(bf16[1024,384]{1,0:T(8,128)(2,1)} %get-tuple-element.17), channel_id=1, source_target_pairs={{0,1},{1,2},{2,3},{3,0},{4,5},{5,6},{6,7},{7,4},{8,9},{9,10},{10,1... | collective-permute-start | bytes 2359304 | tf_op jit(solution)/shard_map/ppermute | solution.py:232
  54.5 3.0 %collective-permute-start.1 = (bf16[1024,384]{1,0:T(8,128)(2,1)}, bf16[1024,384]{1,0:T(8,128)(2,1)S(1)}, u32[]{:S(2)}, u32[]{:S(2)}) collective-permute-start(bf16[1024,384]{1,0:T(8,128)(2,1)} %get-tuple-element.18), channel_id=1, source_target_pairs={{0,2},{1,3},{2,0},{3,1},{4,6},{5,7},{6,4},{7,5},{8,10},{9,11},{10,... | collective-permute-start | bytes 2359304 | tf_op jit(solution)/shard_map/ppermute | solution.py:232
  57.5 4.1 %collective-permute-start.2 = (bf16[1024,384]{1,0:T(8,128)(2,1)}, bf16[1024,384]{1,0:T(8,128)(2,1)}, u32[]{:S(2)}, u32[]{:S(2)}) collective-permute-start(bf16[1024,384]{1,0:T(8,128)(2,1)} %get-tuple-element.19), channel_id=1, source_target_pairs={{0,3},{1,0},{2,1},{3,2},{4,7},{5,4},{6,5},{7,6},{8,11},{9,8},{10,9... | collective-permute-start | bytes 2359304 | tf_op jit(solution)/shard_map/ppermute | solution.py:232
  61.6 10.7 %all-to-all-done.1.x = bf16[16,256,128]{2,1,0:T(8,128)(2,1)S(1)} async-done(((bf16[16,256,128]{2,1,0:T(8,128)(2,1)}), bf16[16,256,128]{2,1,0:T(8,128)(2,1)S(1)}, u32[]{:S(2)}, u32[]{:S(2)}) %all-to-all-start.1) | async-done | bytes 1048608 | tf_op jit(solution)/shard_map/all_to_all | solution.py:26
  72.3 0.3 join.2.x
  72.5 1.0 collective-permute-done.refs_1_
  73.6 5.0 %collective-permute-done.1.refs_2_ = bf16[1024,384]{1,0:T(8,128)(2,1)S(1)} collective-permute-done((bf16[1024,384]{1,0:T(8,128)(2,1)}, bf16[1024,384]{1,0:T(8,128)(2,1)S(1)}, u32[]{:S(2)}, u32[]{:S(2)}) %collective-permute-start.1) | collective-permute-done | bytes 786464 | tf_op jit(solution)/shard_map/ppermute | solution.py:232
  78.5 16.1 %collective-permute-done.2.refs_3_ = bf16[1024,384]{1,0:T(8,128)(2,1)} collective-permute-done((bf16[1024,384]{1,0:T(8,128)(2,1)}, bf16[1024,384]{1,0:T(8,128)(2,1)}, u32[]{:S(2)}, u32[]{:S(2)}) %collective-permute-start.2) | collective-permute-done | bytes 786464 | tf_op jit(solution)/shard_map/ppermute | solution.py:232
  94.6 2.4 %partial_products.2 = bf16[4,512,256]{2,1,0:T(8,128)(2,1)S(1)} custom-call(s32[1]{0:T(128)} %bitcast.at, bf16[512,1024]{1,0:T(8,128)(2,1)S(1)} %join.2.x, bf16[1024,384]{1,0:T(8,128)(2,1)S(1)} %get-tuple-element.16.refs_0_, bf16[1024,384]{1,0:T(8,128)(2,1)S(1)} %collective-permute-done.refs_1_, bf16[1024,384]{1,0:T(8,128)(2,1)S(1)} %collective-permute-done.1.refs_2_, ...), custom_call_target="tpu_custom_call" | custom-call | flops 1073741824 | bytes 4194304 | tf_op jit(solution)/shard_map/partial_products/pallas_call | solution.py:194
  97.0 17.2 %all_to_all.31.p = bf16[4,512,256]{2,1,0:T(8,128)(2,1)S(1)} all-to-all(bf16[4,512,256]{2,1,0:T(8,128)(2,1)S(1)} %partial_products.2), channel_id=1, replica_groups=mesh['z'=16,'c'=2,'y'=8,'x'=4] {'x'}, dimensions={0} | all-to-all | bytes 2097152 | tf_op jit(solution)/shard_map/all_to_all | solution.py:26
  114.2 0.2 hidden_units.1
  114.4 34.0 %all_to_all.32.x = bf16[8,512,128]{2,1,0:T(8,128)(2,1)S(1)} all-to-all(bf16[8,512,128]{2,1,0:T(8,128)(2,1)S(1)} %hidden_units.1), channel_id=1, replica_groups=mesh['z'=16,'c'=2,'y'=8,'x'=4] {'y'}, dimensions={0} | all-to-all | bytes 2097152 | tf_op jit(solution)/shard_map/all_to_all | solution.py:26
  148.4 0.3 join.3.x
  148.7 1.8 %partial_products.3 = bf16[8,256,128]{2,1,0:T(8,128)(2,1)S(1)} custom-call(s32[1]{0:T(128)} %bitcast.at, bf16[512,1024]{1,0:T(8,128)(2,1)S(1)} %join.3.x, bf16[1024,384]{1,0:T(8,128)(2,1)S(1)} %get-tuple-element.16.refs_0_, bf16[1024,384]{1,0:T(8,128)(2,1)S(1)} %collective-permute-done.refs_1_, bf16[1024,384]{1,0:T(8,128)(2,1)S(1)} %collective-permute-done.1.refs_2_, ...), custom_call_target="tpu_custom_call" | custom-call | flops 536870912 | bytes 4194304 | tf_op jit(solution)/shard_map/partial_products/pallas_call | solution.py:194
  150.5 0.0 copy-start.6
  150.5 12.4 %all_to_all.33.p = bf16[8,256,128]{2,1,0:T(8,128)(2,1)S(1)} all-to-all(bf16[8,256,128]{2,1,0:T(8,128)(2,1)S(1)} %partial_products.3), channel_id=1, replica_groups=mesh['z'=16,'c'=2,'y'=8,'x'=4] {'c','x'}, dimensions={0} | all-to-all | bytes 1048576 | tf_op jit(solution)/shard_map/all_to_all | solution.py:26
  162.9 0.1 add_up.1
  163.0 18.3 %all_to_all.34 = bf16[16,32,128]{2,1,0:T(8,128)(2,1)S(1)} all-to-all(bf16[16,32,128]{2,1,0:T(8,128)(2,1)S(1)} %bitcast.17), channel_id=1, replica_groups=mesh['z'=16,'c'=2,'y'=8,'x'=4] {'z'}, dimensions={0} | all-to-all | bytes 262144 | tf_op jit(solution)/shard_map/all_to_all | solution.py:26
  181.3 0.0 copy-done.6
  181.3 0.1 broadcast_in_dim.2.route_ref
  181.4 1.0 combine.1
Async XLA Ops:
  0.0 1.4 copy-start
  1.4 0.7 copy-start.4
  2.1 0.7 copy-start.5
  38.4 8.3 %copy-start.1 = (bf16[1,4096,128]{2,1,0:T(8,128)(2,1)S(1)}, bf16[1,4096,128]{2,1,0:T(8,128)(2,1)}, u32[]{:S(2)}) copy-start(bf16[1,4096,128]{2,1,0:T(8,128)(2,1)} %param.11) | copy-start | bytes 3145732
  39.5 32.8 %all-to-all-start.1 = ((bf16[16,256,128]{2,1,0:T(8,128)(2,1)}), bf16[16,256,128]{2,1,0:T(8,128)(2,1)S(1)}, u32[]{:S(2)}, u32[]{:S(2)}) async-start(bf16[16,256,128]{2,1,0:T(8,128)(2,1)} %fan_out.1), calls=%async_computation.1 | async-start | bytes 2097152 | tf_op jit(solution)/shard_map/all_to_all | solution.py:26
  46.7 1.2 copy-start.2
  47.9 1.2 copy-start.3
  51.1 22.5 %collective-permute-start = (bf16[1024,384]{1,0:T(8,128)(2,1)}, bf16[1024,384]{1,0:T(8,128)(2,1)S(1)}, u32[]{:S(2)}, u32[]{:S(2)}) collective-permute-start(bf16[1024,384]{1,0:T(8,128)(2,1)} %get-tuple-element.17), channel_id=1, source_target_pairs={{0,1},{1,2},{2,3},{3,0},{4,5},{5,6},{6,7},{7,4},{8,9},{9,10},{10,1... | collective-permute-start | bytes 2359304 | tf_op jit(solution)/shard_map/ppermute | solution.py:232
  54.5 24.1 %collective-permute-start.1 = (bf16[1024,384]{1,0:T(8,128)(2,1)}, bf16[1024,384]{1,0:T(8,128)(2,1)S(1)}, u32[]{:S(2)}, u32[]{:S(2)}) collective-permute-start(bf16[1024,384]{1,0:T(8,128)(2,1)} %get-tuple-element.18), channel_id=1, source_target_pairs={{0,2},{1,3},{2,0},{3,1},{4,6},{5,7},{6,4},{7,5},{8,10},{9,11},{10,... | collective-permute-start | bytes 2359304 | tf_op jit(solution)/shard_map/ppermute | solution.py:232
  57.5 37.1 %collective-permute-start.2 = (bf16[1024,384]{1,0:T(8,128)(2,1)}, bf16[1024,384]{1,0:T(8,128)(2,1)}, u32[]{:S(2)}, u32[]{:S(2)}) collective-permute-start(bf16[1024,384]{1,0:T(8,128)(2,1)} %get-tuple-element.19), channel_id=1, source_target_pairs={{0,3},{1,0},{2,1},{3,2},{4,7},{5,4},{6,5},{7,6},{8,11},{9,8},{10,9... | collective-permute-start | bytes 2359304 | tf_op jit(solution)/shard_map/ppermute | solution.py:232
  150.5 30.8 %copy-start.6 = (f32[192,2]{0,1:T(2,128)S(1)}, f32[192,2]{0,1:T(2,128)}, u32[]{:S(2)}) copy-start(f32[192,2]{0,1:T(2,128)} %param.9) | copy-start | bytes 4612

commit v2 on v1

--- a/solution.py
+++ b/solution.py
@@ -77,23 +77,12 @@
     rows, width = tokens.shape
     top = ids.shape[0]
     slots = experts * room
-    chunks = 4 if rows % 64 == 0 else 1
-    step = rows // chunks
-
-    def kernel(at, tok_hbm, ids_hbm, gain_hbm, out, dest_ref, tok, ids_ref, gain_ref, own_ref, sem):
+
+    def kernel(at, tok, ids_ref, gain_ref, out, dest_ref):
+        values = tok[...].astype(F32)
+        scale = lax.rsqrt(jnp.sum(values * values, axis=-1, keepdims=True) * (1.0 / width) + EPS)
         start = pl.multiple_of(at[0] * cols, cols)
-        small = [
-            pltpu.make_async_copy(ids_hbm, ids_ref, sem.at[chunks]),
-            pltpu.make_async_copy(gain_hbm.at[:, pl.ds(start, cols)], gain_ref, sem.at[chunks + 1]),
-        ]
-        large = [
-            pltpu.make_async_copy(tok_hbm.at[pl.ds(i * step, step)], tok.at[pl.ds(i * step, step)], sem.at[i])
-            for i in range(chunks)
-        ]
-        for copy in small + large:
-            copy.start()
-        for copy in small:
-            copy.wait()
+        own = (tok[:, pl.ds(start, cols)].astype(F32) * scale * gain_ref[:, pl.ds(start, cols)]).astype(BF16)
         expert = lax.broadcasted_iota(jnp.int32, (experts, rows), 0)
         here = [ids_ref[k : k + 1, :] == expert for k in range(top)]
         named = sum(h.astype(F32) for h in here).astype(BF16)
@@ -109,60 +98,68 @@
             dest_ref[k : k + 1, :] = dest
             hit = (slot == dest).astype(F32)
             pick = hit if pick is None else pick + hit
-        pick = pick.astype(BF16)
-        for i in range(chunks):
-            large[i].wait()
-            at_rows = slice(i * step, (i + 1) * step)
-            values = tok[at_rows, :].astype(F32)
-            scale = lax.rsqrt(jnp.sum(values * values, axis=-1, keepdims=True) * (1.0 / width) + EPS)
-            own = tok[at_rows, pl.ds(start, cols)].astype(F32)
-            own_ref[at_rows, :] = (own * scale * gain_ref[...]).astype(BF16)
-        out[...] = jnp.dot(pick, own_ref[...], preferred_element_type=F32).astype(BF16)
+        out[...] = jnp.dot(pick.astype(BF16), own, preferred_element_type=F32).astype(BF16)
 
     return pl.pallas_call(
         kernel,
         out_shape=[jax.ShapeDtypeStruct((slots, cols), BF16), jax.ShapeDtypeStruct((top, rows), jnp.int32)],
-        in_specs=[SMEM, HBM, HBM, HBM],
+        in_specs=[SMEM, VMEM, VMEM, VMEM],
         out_specs=[VMEM, VMEM],
-        scratch_shapes=[
-            pltpu.VMEM((rows, width), BF16),
-            pltpu.VMEM((top, rows), jnp.int32),
-            pltpu.VMEM((1, cols), F32),
-            pltpu.VMEM((rows, cols), BF16),
-            pltpu.SemaphoreType.DMA((chunks + 2,)),
-        ],
         compiler_params=params(12),
         name="dispatch",
     )(tp_at, tokens, ids, gain)
 
 
-def fan_out(arrived, copies):
+def by_core(arrived):
     nz, nc, room, cols = arrived.shape
 
     def kernel(x, out):
         for c in range(nc):
-            block = x[:, c].reshape(nz * room, cols)
-            for j in range(copies):
-                out[c * copies + j] = block
-
-    return pl.pallas_call(
-        kernel,
-        out_shape=jax.ShapeDtypeStruct((nc * copies, nz * room, cols), BF16),
+            out[c] = x[:, c].reshape(nz * room, cols)
+
+    return pl.pallas_call(
+        kernel,
+        out_shape=jax.ShapeDtypeStruct((nc, nz * room, cols), BF16),
         in_specs=[VMEM],
         out_specs=VMEM,
         compiler_params=params(4),
-        name="fan_out",
+        name="by_core",
     )(arrived)
 
 
-def join(pieces, groups):
-    blocks, some, cols = pieces.shape
-    rows, ny = some * groups, blocks // groups
+def used_slots(slots, rows, cap, room, slots_first):
+    shape, at = ((slots, rows), 0) if slots_first else ((rows, slots), 1)
+    slot = lax.broadcasted_iota(jnp.int32, shape, at)
+    place = slot & (room - 1)
+    row = lax.shift_right_logical(slot, room.bit_length() - 1) * cap + place
+    hit = (row == lax.broadcasted_iota(jnp.int32, shape, 1 - at)) & (place < cap)
+    return hit.astype(F32).astype(BF16)
+
+
+def close_up(arrived, cap, room):
+    slots, cols = arrived.shape
+    rows = slots // room * cap
 
     def kernel(x, out):
-        for g in range(groups):
-            for j in range(ny):
-                out[g * some : (g + 1) * some, j * cols : (j + 1) * cols] = x[g * ny + j]
+        pick = used_slots(slots, rows, cap, room, False)
+        out[...] = jnp.dot(pick, x[...], preferred_element_type=F32).astype(BF16)
+
+    return pl.pallas_call(
+        kernel,
+        out_shape=jax.ShapeDtypeStruct((rows, cols), BF16),
+        in_specs=[VMEM],
+        out_specs=VMEM,
+        compiler_params=params(4),
+        name="close_up",
+    )(arrived)
+
+
+def join(pieces):
+    ny, rows, cols = pieces.shape
+
+    def kernel(x, out):
+        for j in range(ny):
+            out[:, j * cols : (j + 1) * cols] = x[j]
 
     return pl.pallas_call(
         kernel,
@@ -202,7 +199,7 @@
     )(x_at, left, *weights)
 
 
-def hidden_units(parts, copies):
+def hidden_units(parts):
     nx, rows, wide = parts.shape
     ff = wide // 2
 
@@ -212,13 +209,11 @@
             total += p[j].astype(F32)
         gate = jnp.minimum(total[:, :ff], LIMIT)
         up_part = jnp.clip(total[:, ff:], -LIMIT, LIMIT)
-        hidden = ((up_part + 1.0) * gate * jax.nn.sigmoid(ALPHA * gate)).astype(BF16)
-        for j in range(copies):
-            out[j] = hidden
-
-    return pl.pallas_call(
-        kernel,
-        out_shape=jax.ShapeDtypeStruct((copies, rows, ff), BF16),
+        out[...] = ((up_part + 1.0) * gate * jax.nn.sigmoid(ALPHA * gate)).astype(BF16)
+
+    return pl.pallas_call(
+        kernel,
+        out_shape=jax.ShapeDtypeStruct((rows, ff), BF16),
         in_specs=[VMEM],
         out_specs=VMEM,
         compiler_params=params(8),
@@ -233,20 +228,22 @@
     return [blocks[0]] + [moved[s] for s in range(1, n)]
 
 
-def add_up(parts, groups, blocks):
+def add_up(parts, groups, blocks, cap, room):
     total, rows, cols = parts.shape
     terms = total // groups
 
     def kernel(p, out):
+        spread = used_slots(blocks * room, rows, cap, room, True)
         for g in range(groups):
             value = p[g * terms].astype(F32)
             for j in range(1, terms):
                 value += p[g * terms + j].astype(F32)
-            out[:, g] = value.astype(BF16).reshape(blocks, rows // blocks, cols)
-
-    return pl.pallas_call(
-        kernel,
-        out_shape=jax.ShapeDtypeStruct((blocks, groups, rows // blocks, cols), BF16),
+            value = jnp.dot(spread, value.astype(BF16), preferred_element_type=F32).astype(BF16)
+            out[:, g] = value.reshape(blocks, room, cols)
+
+    return pl.pallas_call(
+        kernel,
+        out_shape=jax.ShapeDtypeStruct((blocks, groups, room, cols), BF16),
         in_specs=[VMEM],
         out_specs=VMEM,
         compiler_params=params(4),
@@ -287,7 +284,7 @@
     top = expert_ids.shape[1]
     experts = nz * nc * gate_weight.shape[0]
     cap = 5 * rows * top // (4 * experts)
-    room = -(-cap // 16) * 16
+    room = max(16, pl.next_power_of_2(cap))
     slots = experts * room
     cols = width // (nx * ny)
     ff = gate_weight.shape[2]
@@ -300,18 +297,18 @@
 
     arrived = swap(buffer.reshape(nz, nc * room, cols), "z").reshape(nz, nc, room, cols)
     weights = from_neighbours(weights, "x")
-    blocks = fan_out(arrived, ny)
-    pieces = swap(blocks, ("c", "y"))
-    left = join(pieces, nc)
+    arrived = by_core(arrived)
+    arrived = swap(arrived, "c").reshape(slots, cols)
+    pieces = lax.all_gather(close_up(arrived, cap, room), "y")
+    left = join(pieces)
     parts = partial_products(at, left, weights, 0, 2 * ff, 1)
     parts = swap(parts, "x")
 
-    hidden = hidden_units(parts, ny)
-    pieces = swap(hidden, "y")
-    parts = partial_products(at, join(pieces, 1), weights, 2 * ff, cols, nc)
+    pieces = lax.all_gather(hidden_units(parts), "y")
+    parts = partial_products(at, join(pieces), weights, 2 * ff, cols, nc)
     parts = swap(parts, ("c", "x"))
 
-    result = add_up(parts, nc, nz).reshape(nz, nc * room, cols)
+    result = add_up(parts, nc, nz, cap, room).reshape(nz, nc * room, cols)
     back = swap(result, "z").reshape(slots, cols)
     return combine(back, dest, jnp.broadcast_to(route_weight.T[:, :, None], (top, rows, cols)))
 

time: 183 us -> 158 us (0.86)
  waiting for transfers between devices: 32.8 us -> 0.01 us
  starting transfers between devices: 17.7 us -> 29.3 us
  Pallas kernels: 11.1 us -> 7.36 us
    all_to_all x5 -> x4, blocking collectives: 115 us -> 58 us  [swap(): return lax.all_to_all(x, axes, split_axis=0, concat_axis=0, tiled=True)]
    all_gather x0 -> x2, blocking collectives: none -> 56.7 us  [the longest x1 28.5 us: on_device(): pieces = lax.all_gather(hidden_units(parts), 'y')]
    ppermute x3, waiting for transfers between devices: 22.1 us -> 0.01 us  [from_neighbours(): moved = {s: lax.ppermute(blocks[s], axis, shifted(n, s)) for s in order}]
    all_to_all x1, starting transfers between devices: 7.2 us -> 18.9 us  [swap(): return lax.all_to_all(x, axes, split_axis=0, concat_axis=0, tiled=True)]
    all_to_all x1, waiting for transfers between devices: 10.7 us -> 0.01 us  [swap(): return lax.all_to_all(x, axes, split_axis=0, concat_axis=0, tiled=True)]
    pallas_call x2, Pallas kernels: 4.23 us -> 1.88 us  [partial_products(): pl.pallas_call(kernel, out_shape=jax.ShapeDtypeStruct((groups * nx, share...]
  transfers between devices with their start and end apart: 4 -> 4, of which waited for: 4 -> 0; matrix products, arithmetic and copies ran while one was open for 0% -> 0% of each run, Pallas kernels for 1% -> 2%
where the time goes in v2:
time: 158 us; the launch traced here: 157 us
  blocking collectives  115 us (73%)
  starting transfers between devices  29.3 us (19%)
  Pallas kernels  7.36 us (5%)
  local copies, waits for them, and re-layouts  5.36 us (3%)
    all_to_all x4, blocking collectives, swap(): return lax.all_to_all(x, axes, split_axis=0, concat_axis=0, tiled=True)  58 us
    all_gather x1, blocking collectives, on_device(): pieces = lax.all_gather(hidden_units(parts), 'y')  28.5 us
    all_gather x1, blocking collectives, on_device(): pieces = lax.all_gather(close_up(arrived, cap, room), 'y')  28.2 us
    all_to_all x1, starting transfers between devices, swap(): return lax.all_to_all(x, axes, split_axis=0, concat_axis=0, tiled=True)  18.9 us
    ppermute x3, starting transfers between devices, from_neighbours(): moved = {s: lax.ppermute(blocks[s], axis, shifted(n, s)) for s in order}  10.5 us
    unnamed x14, local copies, waits for them, and re-layouts  5.26 us
  transfers between devices with their start and end apart: 4, of which 0 were waited for; matrix products, arithmetic and copies ran while one was open for 0% of the time, Pallas kernels for 2%

profile of v2, /device:TPU:2, one launch (start us, length us, event | category | flops | bytes accessed | tf_op | source)
XLA Modules:
  0.0 157.0 jit_solution(10135876610001088895)
XLA Ops:
  0.0 0.0 copy-start
  0.0 1.4 copy-done
  1.4 0.0 copy-start.4
  1.4 0.7 copy-done.4
  2.1 0.0 copy-start.5
  2.1 0.7 copy-done.5
  2.8 0.0 copy-start.1
  2.8 1.3 dispatch.1
  4.1 18.9 %all-to-all-start = ((bf16[16,32,128]{2,1,0:T(8,128)(2,1)}), bf16[16,32,128]{2,1,0:T(8,128)(2,1)S(1)}, u32[]{:S(2)}, u32[]{:S(2)}) async-start(bf16[16,32,128]{2,1,0:T(8,128)(2,1)} %bitcast.4), calls=%async_computation | async-start | bytes 262144 | tf_op jit(solution)/shard_map/all_to_all | solution.py:26
  23.0 0.0 copy-done.1
  23.0 0.0 copy-start.2
  23.0 1.2 copy-done.2
  24.2 0.0 copy-start.3
  24.2 1.2 copy-done.3
  25.4 1.9 %weight_quarters.1 = (bf16[1024,384]{1,0:T(8,128)(2,1)S(1)}, bf16[1024,384]{1,0:T(8,128)(2,1)}, bf16[1024,384]{1,0:T(8,128)(2,1)}, bf16[1024,384]{1,0:T(8,128)(2,1)}) custom-call(s32[1]{0:T(128)} %bitcast.at, bf16[4096,128]{1,0:T(8,128)(2,1)S(1)} %bitcast.17, bf16[4096,128]{1,0:T(8,128)(2,1)S(1)} %bitcast.18, bf16[8,4,128,128]{3,2,1,0:T(8,128)(2,1)S(1)} %bitcast.19), custom_call_target="tpu_custom_call" | custom-call | tf_op jit(solution)/shard_map/weight_quarters/pallas_call | solution.py:65
  27.4 3.4 %collective-permute-start = (bf16[1024,384]{1,0:T(8,128)(2,1)}, bf16[1024,384]{1,0:T(8,128)(2,1)S(1)}, u32[]{:S(2)}, u32[]{:S(2)}) collective-permute-start(bf16[1024,384]{1,0:T(8,128)(2,1)} %get-tuple-element.17), channel_id=1, source_target_pairs={{0,1},{1,2},{2,3},{3,0},{4,5},{5,6},{6,7},{7,4},{8,9},{9,10},{10,1... | collective-permute-start | bytes 2359304 | tf_op jit(solution)/shard_map/ppermute | solution.py:227
  30.8 3.0 %collective-permute-start.1 = (bf16[1024,384]{1,0:T(8,128)(2,1)}, bf16[1024,384]{1,0:T(8,128)(2,1)S(1)}, u32[]{:S(2)}, u32[]{:S(2)}) collective-permute-start(bf16[1024,384]{1,0:T(8,128)(2,1)} %get-tuple-element.18), channel_id=1, source_target_pairs={{0,2},{1,3},{2,0},{3,1},{4,6},{5,7},{6,4},{7,5},{8,10},{9,11},{10,... | collective-permute-start | bytes 2359304 | tf_op jit(solution)/shard_map/ppermute | solution.py:227
  33.8 4.1 %collective-permute-start.2 = (bf16[1024,384]{1,0:T(8,128)(2,1)}, bf16[1024,384]{1,0:T(8,128)(2,1)S(1)}, u32[]{:S(2)}, u32[]{:S(2)}) collective-permute-start(bf16[1024,384]{1,0:T(8,128)(2,1)} %get-tuple-element.19), channel_id=1, source_target_pairs={{0,3},{1,0},{2,1},{3,2},{4,7},{5,4},{6,5},{7,6},{8,11},{9,8},{10,9... | collective-permute-start | bytes 2359304 | tf_op jit(solution)/shard_map/ppermute | solution.py:227
  37.9 0.0 all-to-all-done
  37.9 3.8 %all_to_all.25 = bf16[2,256,128]{2,1,0:T(8,128)(2,1)S(1)} all-to-all(bf16[2,256,128]{2,1,0:T(8,128)(2,1)S(1)} %by_core.1), channel_id=1, replica_groups=mesh['z'=16,'c'=2,'y'=8,'x'=4] {'c'}, dimensions={0} | all-to-all | bytes 262144 | tf_op jit(solution)/shard_map/all_to_all | solution.py:26
  41.7 0.3 close_up.1
  42.0 28.2 %all-gather = bf16[3840,128]{1,0:T(8,128)(2,1)S(1)} all-gather(bf16[480,128]{1,0:T(8,128)(2,1)S(1)} %close_up.1), channel_id=2, replica_groups=mesh['z'=16,'c'=2,'y'=8,'x'=4] {'y'}, dimensions={0}, use_global_device_ids=true | all-gather | bytes 1105920 | tf_op jit(solution)/shard_map/all_gather | solution.py:302
  70.3 0.3 join.2.x
  70.5 0.0 collective-permute-done.refs_1_
  70.6 0.0 collective-permute-done.1.refs_2_
  70.6 0.0 collective-permute-done.2.refs_3_
  70.6 1.2 partial_products.2
  71.8 15.8 %all_to_all.26.p = bf16[4,480,256]{2,1,0:T(8,128)(2,1)S(1)} all-to-all(bf16[4,480,256]{2,1,0:T(8,128)(2,1)S(1)} %partial_products.2), channel_id=1, replica_groups=mesh['z'=16,'c'=2,'y'=8,'x'=4] {'x'}, dimensions={0} | all-to-all | bytes 1966080 | tf_op jit(solution)/shard_map/all_to_all | solution.py:26
  87.6 0.2 hidden_units.1
  87.8 28.5 %all-gather.1 = bf16[3840,128]{1,0:T(8,128)(2,1)S(1)} all-gather(bf16[480,128]{1,0:T(8,128)(2,1)S(1)} %hidden_units.1), channel_id=3, replica_groups=mesh['z'=16,'c'=2,'y'=8,'x'=4] {'y'}, dimensions={0}, use_global_device_ids=true | all-gather | bytes 1105920 | tf_op jit(solution)/shard_map/all_gather | solution.py:307
  116.3 0.3 join.3.x
  116.6 0.7 partial_products.3
  117.3 0.0 copy-start.6
  117.3 12.1 %all_to_all.27.p = bf16[8,240,128]{2,1,0:T(8,128)(2,1)S(1)} all-to-all(bf16[8,240,128]{2,1,0:T(8,128)(2,1)S(1)} %partial_products.3), channel_id=1, replica_groups=mesh['z'=16,'c'=2,'y'=8,'x'=4] {'c','x'}, dimensions={0} | all-to-all | bytes 983040 | tf_op jit(solution)/shard_map/all_to_all | solution.py:26
  129.4 0.3 add_up.1
  129.6 26.2 %all_to_all.28 = bf16[16,32,128]{2,1,0:T(8,128)(2,1)S(1)} all-to-all(bf16[16,32,128]{2,1,0:T(8,128)(2,1)S(1)} %bitcast.21), channel_id=1, replica_groups=mesh['z'=16,'c'=2,'y'=8,'x'=4] {'z'}, dimensions={0} | all-to-all | bytes 262144 | tf_op jit(solution)/shard_map/all_to_all | solution.py:26
  155.9 0.0 copy-done.6
  155.9 0.1 broadcast_in_dim.2.route_ref
  156.0 1.0 combine.1
  (1 shorter events, 0.0 us)
Async XLA Ops:
  0.0 1.4 copy-start
  1.4 0.7 copy-start.4
  2.1 0.7 copy-start.5
  2.8 20.2 %copy-start.1 = (bf16[1,4096,128]{2,1,0:T(8,128)(2,1)S(1)}, bf16[1,4096,128]{2,1,0:T(8,128)(2,1)}, u32[]{:S(2)}) copy-start(bf16[1,4096,128]{2,1,0:T(8,128)(2,1)} %param.11) | copy-start | bytes 3145732
  4.1 33.8 %all-to-all-start = ((bf16[16,32,128]{2,1,0:T(8,128)(2,1)}), bf16[16,32,128]{2,1,0:T(8,128)(2,1)S(1)}, u32[]{:S(2)}, u32[]{:S(2)}) async-start(bf16[16,32,128]{2,1,0:T(8,128)(2,1)} %bitcast.4), calls=%async_computation | async-start | bytes 262144 | tf_op jit(solution)/shard_map/all_to_all | solution.py:26
  23.0 1.2 copy-start.2
  24.2 1.2 copy-start.3
  27.4 43.2 %collective-permute-start = (bf16[1024,384]{1,0:T(8,128)(2,1)}, bf16[1024,384]{1,0:T(8,128)(2,1)S(1)}, u32[]{:S(2)}, u32[]{:S(2)}) collective-permute-start(bf16[1024,384]{1,0:T(8,128)(2,1)} %get-tuple-element.17), channel_id=1, source_target_pairs={{0,1},{1,2},{2,3},{3,0},{4,5},{5,6},{6,7},{7,4},{8,9},{9,10},{10,1... | collective-permute-start | bytes 2359304 | tf_op jit(solution)/shard_map/ppermute | solution.py:227
  30.8 39.8 %collective-permute-start.1 = (bf16[1024,384]{1,0:T(8,128)(2,1)}, bf16[1024,384]{1,0:T(8,128)(2,1)S(1)}, u32[]{:S(2)}, u32[]{:S(2)}) collective-permute-start(bf16[1024,384]{1,0:T(8,128)(2,1)} %get-tuple-element.18), channel_id=1, source_target_pairs={{0,2},{1,3},{2,0},{3,1},{4,6},{5,7},{6,4},{7,5},{8,10},{9,11},{10,... | collective-permute-start | bytes 2359304 | tf_op jit(solution)/shard_map/ppermute | solution.py:227
  33.8 36.8 %collective-permute-start.2 = (bf16[1024,384]{1,0:T(8,128)(2,1)}, bf16[1024,384]{1,0:T(8,128)(2,1)S(1)}, u32[]{:S(2)}, u32[]{:S(2)}) collective-permute-start(bf16[1024,384]{1,0:T(8,128)(2,1)} %get-tuple-element.19), channel_id=1, source_target_pairs={{0,3},{1,0},{2,1},{3,2},{4,7},{5,4},{6,5},{7,6},{8,11},{9,8},{10,9... | collective-permute-start | bytes 2359304 | tf_op jit(solution)/shard_map/ppermute | solution.py:227
  117.3 38.6 %copy-start.6 = (f32[192,2]{0,1:T(2,128)S(1)}, f32[192,2]{0,1:T(2,128)}, u32[]{:S(2)}) copy-start(f32[192,2]{0,1:T(2,128)} %param.9) | copy-start | bytes 4612
